TPU v7x, 256 devices: a 4x2x16 block of a 4x16x16 slice. The times are simulated.
256 devices in a mesh: grp: 2 (over y), sp: 32 (over z, core), tp: 4 (over x).
Axes of the slice: x: 4, y: 2, z: 16, core: 2. Of those that a mesh axis runs over, the one named last changes fastest.
The devices are a block of a 4x16x16 slice.
Arguments:
- query_rows: bfloat16 [8192, 1024], P(('grp', 'sp'), 'tp'), parts along dimension 0, may hold values from -64 to 64
- key_rows: bfloat16 [8192, 512], P(('grp', 'sp'), 'tp'), parts along dimension 0, may hold values from -16 to 16
- value_rows: bfloat16 [8192, 512], P(('grp', 'sp'), 'tp'), parts along dimension 0, may hold values from -6 to 6
- sink_logit: float32 [16], P('tp'), may hold values from 3.5 to 7
- out_weight: bfloat16 [1024, 2048], P('tp'), may hold values from -0.1875 to 0.1875
- residual: bfloat16 [8192, 2048], P(('grp', 'sp', 'tp')), parts along dimension 0, may hold values from -6 to 6
- norm_gain: float32 [2048], replicated, may hold values from 0.1 to 1.9
- routes: int32 [8192, 6], P(('grp', 'sp', 'tp')), parts along dimension 0, may hold values from 0 to 127, as said below
- gate_weights: float32 [8192, 6], P(('grp', 'sp', 'tp')), parts along dimension 0, may hold values from 0.1 to 0.8
- expert_gate: bfloat16 [128, 2048, 512], P(('sp', 'tp')), may hold values from -0.125 to 0.125
- expert_up: bfloat16 [128, 2048, 512], P(('sp', 'tp')), may hold values from -0.125 to 0.125
- expert_down: bfloat16 [128, 512, 2048], P(('sp', 'tp')), may hold values from -0.25 to 0.25
- shared_gate: bfloat16 [2048, 512], P(None, 'tp'), may hold values from -0.125 to 0.125
- shared_up: bfloat16 [2048, 512], P(None, 'tp'), may hold values from -0.125 to 0.125
- shared_down: bfloat16 [512, 2048], P('tp'), may hold values from -0.25 to 0.25
Outputs:
- layer_out: bfloat16 [8192, 2048], P(('grp', 'sp', 'tp')), parts along dimension 0
There are 2 independent parts, one for each index of `grp`. A program takes and returns all parts, laid end to end along the dimension named above; an argument that names none is the same for every part. Nothing has to cross between parts.
Inputs may be any that keep to these rules, and one draw needn't show every extreme that they name: `routes`: in each aligned block of 32 rows (the rows of one device) every row names 6 different experts and no expert is named by more than 3 rows; in every draw some expert is named by exactly 3 rows of every block.
All inputs are finite; a program needn't handle non-finite values.
Results may differ from a plain program's by a relative error of at most 0.015.
Values may be sent and summed in bfloat16 or wider, within the bound.
A program may use at most 64 MiB of HBM per device.

v0:
```python
import jax
import jax.numpy as jnp
from jax import lax
from jax.sharding import PartitionSpec as P

HEAD = 64
WINDOW = 128
TOPK = 6


norm_eps = 1e-06


def with_halo(block, sides, width):
    for axis, dim in sides:
        count = lax.axis_size(axis)
        forward = [(i, i + 1) for i in range(count - 1)]
        backward = [(target, source) for source, target in forward]
        low = lax.ppermute(
            lax.slice_in_dim(block, block.shape[dim] - width, None, axis=dim), axis, forward
        )
        high = lax.ppermute(lax.slice_in_dim(block, 0, width, axis=dim), axis, backward)
        block = jnp.concatenate([low, block, high], axis=dim)
    return block


def in_blocks(x, dim, size):
    before, after = (x.shape[:dim], x.shape[dim + 1 :])
    return jnp.moveaxis(x.reshape(*before, size, -1, *after), dim, 0)


def summed_on_arrival(x, axis, dim):
    size = lax.axis_size(axis)
    parts = lax.all_to_all(in_blocks(x, dim, size), axis, 0, 0, tiled=True)
    return jnp.sum(parts.astype(jnp.float32), axis=0)


def joined_along(parts, dim):
    parts = jnp.moveaxis(parts, 0, dim)
    shape = parts.shape
    return parts.reshape(*shape[:dim], shape[dim] * shape[dim + 1], *shape[dim + 2 :])


def copy_for_each(x, axis):
    size = lax.axis_size(axis)
    return lax.all_to_all(jnp.broadcast_to(x[None], (size, *x.shape)), axis, 0, 0, tiled=True)


def gather_directly(x, axis, dim):
    return joined_along(copy_for_each(x, axis), dim)


def window_attention(query_rows, key_rows, value_rows, sink_logit):
    local_len = query_rows.shape[0]
    head_size = HEAD
    local_kv = key_rows.shape[1] // head_size
    local_heads = query_rows.shape[1] // head_size
    grouped = local_heads // local_kv
    blocks = local_len // WINDOW
    stacked = jnp.stack([key_rows, value_rows])
    widened = with_halo(stacked, (("sp", 1),), WINDOW)
    banded = widened.reshape(2, blocks + 2, WINDOW, local_kv, head_size)
    banded = jnp.concatenate([banded[:, :-2], banded[:, 1:-1], banded[:, 2:]], axis=2)
    queries = query_rows.reshape(blocks, WINDOW, local_kv, grouped, head_size)
    scores = jnp.einsum(
        "nqhgd,nkhd->nhgqk", queries, banded[0], preferred_element_type=jnp.float32
    ) * head_size ** (-0.5)
    seq_start = lax.axis_index("sp") * local_len
    total_len = lax.axis_size("sp") * local_len
    block_ids = jnp.arange(blocks, dtype=jnp.int32)[:, None, None]
    query_pos = seq_start + block_ids * WINDOW + jnp.arange(WINDOW, dtype=jnp.int32)[None, :, None]
    key_pos = (
        seq_start
        + (block_ids - 1) * WINDOW
        + jnp.arange(3 * WINDOW, dtype=jnp.int32)[None, None, :]
    )
    in_window = (jnp.abs(key_pos - query_pos) <= WINDOW) & (key_pos >= 0) & (key_pos < total_len)
    scores = jnp.where(in_window[:, None, None], scores, -jnp.inf)
    sink_part = sink_logit.reshape(1, local_kv, grouped, 1, 1)
    row_max = jnp.maximum(sink_part, jnp.max(scores, axis=-1, keepdims=True))
    shifted = jnp.exp(scores - row_max)
    denominator = jnp.exp(sink_part - row_max) + jnp.sum(shifted, axis=-1, keepdims=True)
    weights = (shifted / denominator).astype(jnp.bfloat16)
    attended = jnp.einsum(
        "nhgqk,nkhd->nqhgd", weights, banded[1], preferred_element_type=jnp.float32
    )
    return attended.astype(jnp.bfloat16).reshape(local_len, local_heads * head_size)


def body(
    query_rows,
    key_rows,
    value_rows,
    sink_logit,
    out_weight,
    residual,
    norm_gain,
    routes,
    gate_weights,
    expert_gate,
    expert_up,
    expert_down,
    shared_gate,
    shared_up,
    shared_down,
):
    attended = window_attention(query_rows, key_rows, value_rows, sink_logit)
    tok_dev = attended.shape[0]
    tok_rows = residual.shape[0]
    model_width = residual.shape[1]
    projected = summed_on_arrival(
        jnp.dot(attended, out_weight, preferred_element_type=jnp.float32).astype(jnp.bfloat16),
        "tp",
        0,
    )
    stream = residual.astype(jnp.float32) + projected
    normed = (
        stream * lax.rsqrt(jnp.mean(stream * stream, axis=-1, keepdims=True) + norm_eps) * norm_gain
    ).astype(jnp.bfloat16)
    sp_count = lax.axis_size("sp")
    tp_count = lax.axis_size("tp")
    experts_all = sp_count * tp_count
    capacity = (2 * tok_dev * TOPK + tp_count * experts_all - 1) // (tp_count * experts_all)
    copies = tok_rows * TOPK
    flat_expert = routes.reshape(-1)
    one_hot = (flat_expert[:, None] == jnp.arange(experts_all, dtype=jnp.int32)[None, :]).astype(
        jnp.int32
    )
    rank_in_expert = jnp.sum(jnp.cumsum(one_hot, axis=0) * one_hot, axis=1) - 1
    target_slot = flat_expert * capacity + rank_in_expert
    slot_token = (
        jnp.full((experts_all * capacity,), tok_rows, jnp.int32)
        .at[target_slot]
        .set(jnp.arange(copies, dtype=jnp.int32) // TOPK)
    )
    padded_rows = jnp.concatenate([normed, jnp.zeros((1, model_width), jnp.bfloat16)], axis=0)
    outgoing = padded_rows[slot_token].reshape(experts_all, capacity, model_width)
    incoming = lax.all_to_all(outgoing, ("sp", "tp"), split_axis=0, concat_axis=0, tiled=True)
    shaped = incoming.reshape(-1, model_width)
    gate_part = jnp.dot(shaped, expert_gate[0], preferred_element_type=jnp.float32)
    up_part = jnp.dot(shaped, expert_up[0], preferred_element_type=jnp.float32)
    hidden = (jax.nn.silu(gate_part) * up_part).astype(jnp.bfloat16)
    result = jnp.dot(hidden, expert_down[0], preferred_element_type=jnp.float32).astype(
        jnp.bfloat16
    )
    returned = lax.all_to_all(
        result.reshape(incoming.shape), ("sp", "tp"), split_axis=0, concat_axis=0, tiled=True
    )
    returned = returned.reshape(experts_all * capacity, model_width)
    gathered_copies = returned[target_slot].reshape(tok_rows, TOPK, model_width)
    routed = jnp.sum(gate_weights[:, :, None] * gathered_copies.astype(jnp.float32), axis=1)
    slab_rows = gather_directly(normed, "tp", 0)
    gate_part = jnp.dot(slab_rows, shared_gate, preferred_element_type=jnp.float32)
    up_part = jnp.dot(slab_rows, shared_up, preferred_element_type=jnp.float32)
    hidden = (jax.nn.silu(gate_part) * up_part).astype(jnp.bfloat16)
    partials = jnp.dot(hidden, shared_down, preferred_element_type=jnp.float32)
    shared = summed_on_arrival(partials.astype(jnp.bfloat16), "tp", 0)
    return (stream + routed + shared).astype(jnp.bfloat16)


def solution(mesh):
    placed = (
        P(("grp", "sp"), "tp"),
        P(("grp", "sp"), "tp"),
        P(("grp", "sp"), "tp"),
        P("tp"),
        P("tp", None),
        P(("grp", "sp", "tp"), None),
        P(),
        P(("grp", "sp", "tp"), None),
        P(("grp", "sp", "tp"), None),
        P(("sp", "tp"), None, None),
        P(("sp", "tp"), None, None),
        P(("sp", "tp"), None, None),
        P(None, "tp"),
        P(None, "tp"),
        P("tp", None),
    )
    return jax.shard_map(
        body, mesh=mesh, in_specs=placed, out_specs=P(("grp", "sp", "tp"), None), check_vma=False
    )
```

profile of v0, /device:TPU:40, one launch (start us, length us, event | category | flops | bytes accessed | tf_op | source)
XLA Modules:
  0.0 319.7 jit_solution(16336411111788215835)
XLA Ops:
  0.9 1.8 collective-permute-start
  2.8 1.3 collective-permute-start.1
  11.6 1.1 convolution_convert_fusion.2
  12.7 4.6 %all-to-all-start = ((bf16[4,32,2048]{2,1,0:T(8,128)(2,1)}), bf16[4,32,2048]{2,1,0:T(8,128)(2,1)S(1)}, u32[]{:S(2)}, u32[]{:S(2)}) async-start(bf16[4,32,2048]{2,1,0:T(8,128)(2,1)} %bitcast.15), calls=%async_computation | async-start | bytes 1048576 | tf_op jit(solution)/shard_map/all_to_all | solution.py:34
  17.3 8.6 %all-to-all-done = bf16[4,32,2048]{2,1,0:T(8,128)(2,1)S(1)} async-done(((bf16[4,32,2048]{2,1,0:T(8,128)(2,1)}), bf16[4,32,2048]{2,1,0:T(8,128)(2,1)S(1)}, u32[]{:S(2)}, u32[]{:S(2)}) %all-to-all-start) | async-done | bytes 524320 | tf_op jit(solution)/shard_map/all_to_all | solution.py:34
  27.1 3.6 %all-to-all-start.3 = ((bf16[4,32,2048]{2,1,0:T(8,128)(2,1)}), bf16[4,32,2048]{2,1,0:T(8,128)(2,1)S(1)}, u32[]{:S(2)}, u32[]{:S(2)}) async-start(bf16[4,32,2048]{2,1,0:T(8,128)(2,1)} %broadcast_in_dim.22), calls=%async_computation.3 | async-start | bytes 1048576 | tf_op jit(solution)/shard_map/all_to_all | solution.py:46
  30.7 1.2 scatter_custom_fusion
  31.9 3.1 gather_fusion
  35.1 5.1 %reshape.263 = bf16[128,3,2048]{2,1,0:T(4,128)(2,1)} reshape(bf16[384,2048]{1,0:T(8,128)(2,1)} %gather_fusion) | data formatting | bytes 3145728 | tf_op jit(solution)/shard_map/reshape | solution.py:137
  40.3 36.1 %all-to-all-start.1 = ((bf16[128,3,2048]{2,1,0:T(4,128)(2,1)}), bf16[128,3,2048]{2,1,0:T(4,128)(2,1)}, u32[]{:S(2)}, u32[]{:S(2)}) async-start(bf16[128,3,2048]{2,1,0:T(4,128)(2,1)} %reshape.263), calls=%async_computation.1 | async-start | bytes 4194304 | tf_op jit(solution)/shard_map/all_to_all | solution.py:138
  76.4 1.3 fusion.43
  77.8 2.5 convolution_convert_fusion.1
  80.3 91.9 %all-to-all-done.1 = bf16[128,3,2048]{2,1,0:T(4,128)(2,1)} async-done(((bf16[128,3,2048]{2,1,0:T(4,128)(2,1)}), bf16[128,3,2048]{2,1,0:T(4,128)(2,1)}, u32[]{:S(2)}, u32[]{:S(2)}) %all-to-all-start.1) | async-done | bytes 1572896 | tf_op jit(solution)/shard_map/all_to_all | solution.py:138
  172.1 3.7 %all-to-all-start.4 = ((bf16[4,32,2048]{2,1,0:T(8,128)(2,1)}), bf16[4,32,2048]{2,1,0:T(8,128)(2,1)S(1)}, u32[]{:S(2)}, u32[]{:S(2)}) async-start(bf16[4,32,2048]{2,1,0:T(8,128)(2,1)} %bitcast.74), calls=%async_computation.4 | async-start | bytes 1048576 | tf_op jit(solution)/shard_map/all_to_all | solution.py:34
  175.9 5.0 %reshape.264 = bf16[384,2048]{1,0:T(8,128)(2,1)} reshape(bf16[128,3,2048]{2,1,0:T(4,128)(2,1)} %all-to-all-done.1) | data formatting | bytes 3145728 | tf_op jit(solution)/shard_map/reshape | solution.py:139
  180.9 3.9 %fusion.3 = f32[384,512]{1,0:T(8,128)} fusion(bf16[384,2048]{1,0:T(8,128)(2,1)} %reshape.264, bf16[1,2048,512]{2,1,0:T(8,128)(2,1)} %param.24), kind=kOutput, calls=%fused_computation.9 | convolution fusion | flops 805306368 | bytes 4456448 | tf_op jit(solution)/shard_map/dot_general | solution.py:140
  184.9 5.3 %convolution_convert_fusion = bf16[384,2048]{1,0:T(8,128)(2,1)} fusion(bf16[1,512,2048]{2,1,0:T(8,128)(2,1)S(1)} %copy-done, bf16[384,2048]{1,0:T(8,128)(2,1)} %reshape.264, bf16[1,2048,512]{2,1,0:T(8,128)(2,1)} %param.25, f32[384,512]{1,0:T(8,128)} %fusion.3), kind=kOutput, calls=%fused_computation.3 | convolution fusion | flops 1612578816 | bytes 8126464 | tf_op jit(solution)/shard_map/dot_general | solution.py:143
  190.2 5.1 %reshape.265 = bf16[128,3,2048]{2,1,0:T(4,128)(2,1)} reshape(bf16[384,2048]{1,0:T(8,128)(2,1)} %convolution_convert_fusion) | data formatting | bytes 3145728 | tf_op jit(solution)/shard_map/reshape | solution.py:147
  195.3 13.6 %all-to-all-start.2 = ((bf16[128,3,2048]{2,1,0:T(4,128)(2,1)}), bf16[128,3,2048]{2,1,0:T(4,128)(2,1)}, u32[]{:S(2)}, u32[]{:S(2)}) async-start(bf16[128,3,2048]{2,1,0:T(4,128)(2,1)} %reshape.265), calls=%async_computation.2 | async-start | bytes 4194304 | tf_op jit(solution)/shard_map/all_to_all | solution.py:146
  209.8 94.8 %all-to-all-done.2 = bf16[128,3,2048]{2,1,0:T(4,128)(2,1)} async-done(((bf16[128,3,2048]{2,1,0:T(4,128)(2,1)}), bf16[128,3,2048]{2,1,0:T(4,128)(2,1)}, u32[]{:S(2)}, u32[]{:S(2)}) %all-to-all-start.2) | async-done | bytes 1572896 | tf_op jit(solution)/shard_map/all_to_all | solution.py:146
  304.6 5.0 %reshape.266 = bf16[384,2048]{1,0:T(8,128)(2,1)} reshape(bf16[128,3,2048]{2,1,0:T(4,128)(2,1)} %all-to-all-done.2) | data formatting | bytes 3145728 | tf_op jit(solution)/shard_map/reshape | solution.py:149
  309.7 4.4 %gather_fusion.1 = bf16[192,2048]{1,0:T(8,128)(2,1)} fusion(bf16[384,2048]{1,0:T(8,128)(2,1)} %reshape.266, s32[1024]{0:T(1024)S(1)} %pad_clamp_fusion), kind=kCustom, calls=%fused_computation.1 | custom fusion | bytes 1573632 | tf_op jit(solution)/shard_map/gather | solution.py:150
  314.1 2.6 reshape.270
  316.6 2.3 multiply_reduce_fusion
  (65 shorter events, 11.2 us)
Async XLA Ops:
  0.0 184.9 %copy-start = (bf16[1,512,2048]{2,1,0:T(8,128)(2,1)S(1)}, bf16[1,512,2048]{2,1,0:T(8,128)(2,1)}, u32[]{:S(2)}) copy-start(bf16[1,512,2048]{2,1,0:T(8,128)(2,1)} %param.26) | copy-start | bytes 6291460
  0.9 7.4 %collective-permute-start = (bf16[2,128,128]{2,1,0:T(8,128)(2,1)S(1)}, bf16[2,128,128]{2,1,0:T(8,128)(2,1)S(1)}, u32[]{:S(2)}, u32[]{:S(2)}) collective-permute-start(bf16[2,128,128]{2,1,0:T(8,128)(2,1)S(1)} %pad_maximum_fusion.2), channel_id=1, source_target_pairs={{0,4},{4,8},{8,12},{12,16},{16,20},{20,24},{24,28},{28,32},{32,36}... | collective-permute-start | bytes 196616 | tf_op jit(solution)/shard_map/ppermute | solution.py:19
  2.8 5.7 %collective-permute-start.1 = (bf16[2,128,128]{2,1,0:T(8,128)(2,1)S(1)}, bf16[2,128,128]{2,1,0:T(8,128)(2,1)S(1)}, u32[]{:S(2)}, u32[]{:S(2)}) collective-permute-start(bf16[2,128,128]{2,1,0:T(8,128)(2,1)S(1)} %pad_maximum_fusion.2), channel_id=1, source_target_pairs={{4,0},{8,4},{12,8},{16,12},{20,16},{24,20},{28,24},{32,28},{36,32}... | collective-permute-start | bytes 196616 | tf_op jit(solution)/shard_map/ppermute | solution.py:22
  10.4 1.2 copy-start.2
  11.0 15.0 %copy-start.1 = (bf16[32,2048]{1,0:T(8,128)(2,1)S(1)}, bf16[32,2048]{1,0:T(8,128)(2,1)}, u32[]{:S(2)}) copy-start(bf16[32,2048]{1,0:T(8,128)(2,1)} %param.20) | copy-start | bytes 393220
  11.0 15.2 %copy-start.4 = (f32[2048]{0:T(1024)S(1)}, f32[2048]{0:T(1024)}, u32[]{:S(2)}) copy-start(f32[2048]{0:T(1024)} %param.21) | copy-start | bytes 24580
  12.7 13.1 %all-to-all-start = ((bf16[4,32,2048]{2,1,0:T(8,128)(2,1)}), bf16[4,32,2048]{2,1,0:T(8,128)(2,1)S(1)}, u32[]{:S(2)}, u32[]{:S(2)}) async-start(bf16[4,32,2048]{2,1,0:T(8,128)(2,1)} %bitcast.15), calls=%async_computation | async-start | bytes 1048576 | tf_op jit(solution)/shard_map/all_to_all | solution.py:34
  27.1 13.2 %all-to-all-start.3 = ((bf16[4,32,2048]{2,1,0:T(8,128)(2,1)}), bf16[4,32,2048]{2,1,0:T(8,128)(2,1)S(1)}, u32[]{:S(2)}, u32[]{:S(2)}) async-start(bf16[4,32,2048]{2,1,0:T(8,128)(2,1)} %broadcast_in_dim.22), calls=%async_computation.3 | async-start | bytes 1048576 | tf_op jit(solution)/shard_map/all_to_all | solution.py:46
  40.3 131.8 %all-to-all-start.1 = ((bf16[128,3,2048]{2,1,0:T(4,128)(2,1)}), bf16[128,3,2048]{2,1,0:T(4,128)(2,1)}, u32[]{:S(2)}, u32[]{:S(2)}) async-start(bf16[128,3,2048]{2,1,0:T(4,128)(2,1)} %reshape.263), calls=%async_computation.1 | async-start | bytes 4194304 | tf_op jit(solution)/shard_map/all_to_all | solution.py:138
  172.1 23.2 %all-to-all-start.4 = ((bf16[4,32,2048]{2,1,0:T(8,128)(2,1)}), bf16[4,32,2048]{2,1,0:T(8,128)(2,1)S(1)}, u32[]{:S(2)}, u32[]{:S(2)}) async-start(bf16[4,32,2048]{2,1,0:T(8,128)(2,1)} %bitcast.74), calls=%async_computation.4 | async-start | bytes 1048576 | tf_op jit(solution)/shard_map/all_to_all | solution.py:34
  195.3 13.6 %copy-start.5 = (f32[32,6]{0,1:T(8,128)S(1)}, f32[32,6]{0,1:T(8,128)}, u32[]{:S(2)}) copy-start(f32[32,6]{0,1:T(8,128)} %param.23) | copy-start | bytes 2308
  195.3 109.3 %all-to-all-start.2 = ((bf16[128,3,2048]{2,1,0:T(4,128)(2,1)}), bf16[128,3,2048]{2,1,0:T(4,128)(2,1)}, u32[]{:S(2)}, u32[]{:S(2)}) async-start(bf16[128,3,2048]{2,1,0:T(4,128)(2,1)} %reshape.265), calls=%async_computation.2 | async-start | bytes 4194304 | tf_op jit(solution)/shard_map/all_to_all | solution.py:146
  314.1 4.9 %copy-start.3 = (f32[32,2048]{1,0:T(8,128)S(1)}, f32[32,2048]{1,0:T(8,128)}, u32[]{:S(2)}) copy-start(f32[32,2048]{1,0:T(8,128)} %convert_reduce_fusion) | copy-start | bytes 786436
where the time goes:
time: 322 us; the launch traced here: 320 us
  waiting for transfers between devices  195 us (61%)
  starting transfers between devices  64.7 us (20%)
  local copies, waits for them, and re-layouts  36.8 us (11%)
  matrix products  14.8 us (5%)
  other arithmetic  7.61 us (2%)
    all_to_all x1, waiting for transfers between devices, body(): lax.all_to_all(result.reshape(incoming.shape), ('sp', 'tp'), split_axis=0...  94.8 us
    all_to_all x1, waiting for transfers between devices, body(): lax.all_to_all(outgoing, ('sp', 'tp'), split_axis=0, concat_axis=0, tiled...  91.9 us
    all_to_all x1, starting transfers between devices, body(): lax.all_to_all(outgoing, ('sp', 'tp'), split_axis=0, concat_axis=0, tiled...  36.1 us
    all_to_all x1, starting transfers between devices, body(): lax.all_to_all(result.reshape(incoming.shape), ('sp', 'tp'), split_axis=0...  13.6 us
    all_to_all x2, waiting for transfers between devices, summed_on_arrival(): parts = lax.all_to_all(in_blocks(x, dim, size), axis, 0, 0, tiled=True)  8.56 us
    all_to_all x2, starting transfers between devices, summed_on_arrival(): parts = lax.all_to_all(in_blocks(x, dim, size), axis, 0, 0, tiled=True)  8.31 us
  transfers between devices with their start and end apart: 7, of which 5 were waited for; matrix products, arithmetic and copies ran while one was open for 12% of the time, Pallas kernels for 0%

commit v1 on v0

v1 whole, which is shorter than its diff:
```python
import functools

import jax
import jax.numpy as jnp
from jax import lax
from jax.experimental import pallas as pl
from jax.experimental.pallas import tpu as pltpu
from jax.sharding import PartitionSpec as P

HEAD = 64
WINDOW = 128
TOPK = 6
CAP = 3
NCH = 4
PER = 5
NORM_EPS = 1e-06
MESH = pl.DeviceIdType.MESH
F32 = jnp.float32
BF16 = jnp.bfloat16


def iota(shape, dim):
    return lax.broadcasted_iota(jnp.int32, shape, dim)


def dot(a, b):
    return jnp.dot(a, b, preferred_element_type=F32)


def silu(v):
    return v / (1.0 + jnp.exp(-v))


def kernel(
    nz,
    nx,
    q_hbm,
    k_hbm,
    v_hbm,
    sink_ref,
    ow_hbm,
    res_hbm,
    gain_ref,
    routes_ref,
    gw_ref,
    eg_hbm,
    eu_hbm,
    ed_hbm,
    sg_hbm,
    su_hbm,
    sd_hbm,
    out_ref,
    qb,
    kv,
    ow,
    res,
    eg,
    eu,
    ed,
    wsh,
    sd,
    att,
    pbuf,
    precv,
    stream,
    slab,
    shp,
    shr,
    ag,
    meta,
    sel,
    com,
    sb,
    rb,
    eo,
    cb,
    part,
    own,
    rsr,
    rss,
    lsem,
    hsend,
    hrecv,
    psend,
    pecv,
    nsend,
    nrecv,
    ssend,
    srecv,
    agsend,
    agrecv,
    msend,
    mrecv,
    dsend,
    drecv,
    csend,
    crecv,
    rsend,
    rrecv,
):
    rows, width = res.shape
    cw = width // NCH
    half = nz // 2
    plane = 2 * nx
    groups = (nz - 1) // PER
    group_rows = PER * CAP + 1
    order = [0]
    for k in range(1, half):
        order += [k, -k]
    order.append(half)
    slot = {d: i for i, d in enumerate(order)}
    slot[-half] = slot[half]

    sp = lax.axis_index("sp")
    x = lax.axis_index("tp")
    nsp = 2 * nz
    z = sp // 2
    c = sp % 2
    zs = ((z + 1) % nz, (z + nz - 1) % nz)

    def at(z_, c_, x_):
        return {"sp": z_ * 2 + c_, "tp": x_}

    def mate(q):
        dc, dx = q // nx, q % nx
        return (c if dc == 0 else 1 - c), (x + dx) % nx

    def back(q):
        dc, dx = q // nx, q % nx
        return dc * nx + (nx - dx) % nx

    sent = []

    def send(src, dst, ss, rs, device):
        copy = pltpu.make_async_remote_copy(
            src_ref=src,
            dst_ref=dst,
            send_sem=ss,
            recv_sem=rs,
            device_id=device,
            device_id_type=MESH,
        )
        copy.start()
        sent.append(copy)

    me = at(z, c, x)

    def arrived(dst, rs):
        pltpu.make_async_remote_copy(
            src_ref=dst,
            dst_ref=dst,
            send_sem=rs,
            recv_sem=rs,
            device_id=me,
            device_id_type=MESH,
        ).wait_recv()

    barrier = pltpu.get_barrier_semaphore()
    cross = at((z + nz + 2 * c - 1) % nz, 1 - c, x)
    friends = [cross, at(zs[0], c, x), at(zs[1], c, x)]
    for q in range(1, plane):
        cq, xq = mate(q)
        friends.append(at(z, cq, xq))
    for friend in friends:
        pl.semaphore_signal(barrier, inc=1, device_id=friend, device_id_type=MESH)

    loads = []

    def load(src, dst):
        copy = pltpu.make_async_copy(src, dst, lsem.at[len(loads)])
        copy.start()
        loads.append(copy)
        return copy

    span = kv.shape[1] // 3
    load_k = load(k_hbm, kv.at[0, span : 2 * span])
    load_v = load(v_hbm, kv.at[1, span : 2 * span])
    load_q = load(q_hbm, qb)
    load_ow = load(ow_hbm, ow)
    load_res = load(res_hbm, res)
    unit = sg_hbm.shape[1]
    load_sg = load(sg_hbm, wsh.at[:, 0:unit])
    load_su = load(su_hbm, wsh.at[:, unit : 2 * unit])
    load_sd = load(sd_hbm, sd)
    load_eg = load(eg_hbm.at[0], eg)
    load_eu = load(eu_hbm.at[0], eu)
    load_ed = load(ed_hbm.at[0], ed)

    lane = iota((rows, 128), 1)
    ids = routes_ref[...]
    gates = gw_ref[...]
    hot = jnp.zeros((rows, 128), F32)
    for k in range(TOPK):
        hot = hot + jnp.where(lane == ids[:, k : k + 1], 1.0, 0.0)
    below = jnp.where(iota((rows, rows), 0) > iota((rows, rows), 1), 1.0, 0.0)
    before = dot(below.astype(BF16), hot.astype(BF16))
    e_cols = jnp.full((rows, 128), -1.0, F32)
    r_cols = jnp.zeros((rows, 128), F32)
    g_cols = jnp.zeros((rows, 128), F32)
    for k in range(TOPK):
        e_k = ids[:, k : k + 1]
        rank = jnp.sum(jnp.where(lane == e_k, before, 0.0), axis=1, keepdims=True)
        here = lane == k
        e_cols = jnp.where(here, e_k.astype(F32), e_cols)
        r_cols = jnp.where(here, rank, r_cols)
        g_cols = jnp.where(here, gates[:, k : k + 1], g_cols)
    spread = jnp.where((lane & (rows - 1)) == iota((rows, 128), 0), 1.0, 0.0).astype(BF16)

    def on_lanes(cols):
        return dot(cols.T.astype(BF16), spread)[0:8]

    g_high = g_cols.astype(BF16).astype(F32)
    meta[0, 0:8, :] = 4.0 * on_lanes(e_cols) + on_lanes(r_cols)
    meta[0, 8:16, :] = on_lanes(g_high) + on_lanes(g_cols - g_high)

    load_k.wait()
    load_v.wait()
    pl.semaphore_wait(barrier, len(friends))

    mine = kv.at[:, span : 2 * span, :]
    nxt = {"sp": (sp + 1) % nsp, "tp": x}
    prv = {"sp": (sp + nsp - 1) % nsp, "tp": x}
    send(mine, kv.at[:, 0:span, :], hsend.at[0], hrecv.at[0], nxt)
    send(mine, kv.at[:, 2 * span : 3 * span, :], hsend.at[1], hrecv.at[1], prv)

    load_q.wait()
    lane_q = iota((span, 128), 1)
    low = lane_q < HEAD
    heads = []
    for h in range(2 * (qb.shape[1] // 128)):
        pair = qb[:, (h // 2) * 128 : (h // 2) * 128 + 128].astype(F32)
        if h % 2 != h // 2:
            pair = pltpu.roll(pair, HEAD, 1)
        keep = low if h // 2 == 0 else jnp.logical_not(low)
        heads.append(jnp.where(keep, pair, 0.0).astype(BF16))

    row_i = iota((span, 3 * span), 0)
    col_i = iota((span, 3 * span), 1)
    pos = sp * span - span + col_i
    open_ = (col_i >= row_i) & (col_i <= row_i + 2 * WINDOW) & (pos >= 0) & (pos < nsp * span)
    arrived(kv.at[:, 0:span, :], hrecv.at[0])
    arrived(kv.at[:, 2 * span : 3 * span, :], hrecv.at[1])
    keys = kv[0]
    values = kv[1]
    results = []
    for h, query in enumerate(heads):
        scores = lax.dot_general(
            query, keys, (((1,), (1,)), ((), ())), preferred_element_type=F32
        ) * (HEAD**-0.5)
        scores = jnp.where(open_, scores, -jnp.inf)
        sink = sink_ref[h]
        row_max = jnp.maximum(jnp.max(scores, axis=-1, keepdims=True), sink)
        shifted = jnp.exp(scores - row_max)
        denominator = jnp.exp(sink - row_max) + jnp.sum(shifted, axis=-1, keepdims=True)
        weights = (shifted / denominator).astype(BF16)
        got = dot(weights, values)
        if h % 2 != h // 2:
            got = pltpu.roll(got, HEAD, 1)
        results.append(got)
    for pair in range(len(heads) // 2):
        att[:, pair * 128 : pair * 128 + 128] = jnp.where(
            low, results[2 * pair], results[2 * pair + 1]
        ).astype(BF16)

    load_ow.wait()
    attended = att[...]
    for ch in range(NCH):
        cols = slice(ch * cw, (ch + 1) * cw)
        pbuf[:, cols] = dot(attended, ow[:, cols]).astype(BF16)
    for dx in (2, 1, 3):
        xq = (x + dx) % nx
        there = (nx - dx) % nx
        begin = pl.multiple_of(xq * rows, rows)
        send(
            pbuf.at[pl.ds(begin, rows), :],
            precv.at[there],
            psend.at[dx],
            pecv.at[there],
            at(z, c, xq),
        )
    load_res.wait()
    total = res[...].astype(F32) + pbuf[pl.ds(pl.multiple_of(x * rows, rows), rows), :].astype(F32)
    for dx in range(1, nx):
        arrived(precv.at[dx], pecv.at[dx])
    for dx in range(1, nx):
        total = total + precv[dx].astype(F32)
    stream[...] = total
    scale = lax.rsqrt(jnp.mean(total * total, axis=-1, keepdims=True) + NORM_EPS)
    normed = (total * scale * gain_ref[...]).astype(BF16)
    slab[0:rows, :] = normed
    for ch in range(NCH):
        ag[ch, 0:rows, :] = normed[:, ch * cw : (ch + 1) * cw]

    def carries(direction, step, ch):
        return step < half or (step == half and (ch < NCH // 2) == (direction == 0))

    def source(direction, step):
        return slot[-step if direction == 0 else step]

    def block(ch, s):
        return ag.at[ch, s * rows : (s + 1) * rows, :]

    def forward(step, ch, direction):
        if not carries(direction, step, ch):
            return
        a, b = source(direction, step - 1), source(direction, step)
        send(
            block(ch, a),
            block(ch, b),
            agsend.at[direction, step - 1, ch],
            agrecv.at[b, ch],
            at(zs[direction], c, x),
        )

    def forward_meta(step, direction):
        if step == half and direction == 1:
            return
        a, b = source(direction, step - 1), source(direction, step)
        send(
            meta.at[a],
            meta.at[b],
            msend.at[direction, step - 1],
            mrecv.at[b],
            at(zs[direction], c, x),
        )

    def gather_step(step):
        for ch in range(NCH):
            for direction in range(2):
                if carries(direction, step, ch):
                    s = source(direction, step)
                    arrived(block(ch, s), agrecv.at[s, ch])
                    if step < half:
                        forward(step + 1, ch, direction)
        for direction in range(2):
            if not (step == half and direction == 1):
                s = source(direction, step)
                arrived(meta.at[s], mrecv.at[s])
                if step < half:
                    forward_meta(step + 1, direction)

    for ch in range(NCH):
        for direction in range(2):
            forward(1, ch, direction)
    for direction in range(2):
        forward_meta(1, direction)
    for dx in (2, 1, 3):
        there = (nx - dx) % nx
        send(
            slab.at[0:rows, :],
            slab.at[there * rows : (there + 1) * rows, :],
            nsend.at[dx],
            nrecv.at[there],
            at(z, c, (x + dx) % nx),
        )

    def shared_expert():
        for dx in range(1, nx):
            arrived(slab.at[dx * rows : (dx + 1) * rows, :], nrecv.at[dx])
        load_sg.wait()
        load_su.wait()
        load_sd.wait()
        both = dot(slab[...], wsh[...])
        hidden = (silu(both[:, 0:unit]) * both[:, unit : 2 * unit]).astype(BF16)
        for ch in range(NCH):
            cols = slice(ch * cw, (ch + 1) * cw)
            shp[:, cols] = dot(hidden, sd[:, cols]).astype(BF16)
        for dx in (2, 1, 3):
            there = (nx - dx) % nx
            send(
                shp.at[dx * rows : (dx + 1) * rows, :],
                shr.at[there],
                ssend.at[dx],
                srecv.at[there],
                at(z, c, (x + dx) % nx),
            )

    def build(g):
        lane8 = iota((8, 128), 1)
        seg8 = lane8 // rows
        codes, gws = [], []
        for v in range(2):
            code = jnp.full((8, 128), -4.0, F32)
            gate = jnp.zeros((8, 128), F32)
            for i in range(4):
                p = 4 * v + i
                if p > PER:
                    continue
                s = 0 if p == 0 else PER * g + p
                code = jnp.where(seg8 == i, meta[s, 0:8, :], code)
                gate = jnp.where(seg8 == i, meta[s, 8:16, :], gate)
            codes.append(code)
            gws.append(gate)
        rr = iota((group_rows, 128), 0)
        bi = (rr * 11) >> 5
        last = rr == group_rows - 1
        pos_r = jnp.where(last, 0, 1 + bi)
        rank_r = jnp.where(last, g, rr - 3 * bi)
        seg = iota((group_rows, 128), 1) // rows
        turned = []
        for q in range(plane):
            cq, xq = mate(q)
            expert = plane * z + nx * cq + xq
            want = (rank_r + 4 * expert).astype(F32)
            lines = []
            for v in range(2):
                placed = pos_r == seg + 4 * v
                one = jnp.zeros((group_rows, 128), F32)
                weight = jnp.zeros((group_rows, 128), F32)
                for k in range(TOPK):
                    match = (codes[v][k : k + 1, :] == want) & placed
                    one = jnp.where(match, 1.0, one)
                    weight = jnp.where(match, gws[v][k : k + 1, :], weight)
                sel[g, q * group_rows : (q + 1) * group_rows, v * 128 : (v + 1) * 128] = one.astype(
                    BF16
                )
                lines.append(weight)
            turned.append(lines)
        for v in range(2):
            column = jnp.concatenate([turned[q][v] for q in range(plane)], axis=0)
            com[g, v * 128 : (v + 1) * 128, :] = column.T.astype(BF16)

    def dispatch(g):
        build(g)
        choose = sel[g]
        for ch in range(NCH):
            cols = slice(ch * cw, (ch + 1) * cw)
            first = ag[ch, 0:rows, :]
            begin = (1 + PER * g) * rows
            stack = jnp.concatenate(
                [first, ag[ch, begin : begin + PER * rows, :], first, first], axis=0
            )
            picked = dot(choose, stack).astype(BF16)
            rb[g, 0:group_rows, cols] = picked[0:group_rows]
            sb[g, group_rows:, cols] = picked[group_rows:]
        for q in far:
            cq, xq = mate(q)
            b = back(q)
            send(
                sb.at[g, q * group_rows : (q + 1) * group_rows, :],
                rb.at[g, b * group_rows : (b + 1) * group_rows, :],
                dsend.at[g, q],
                drecv.at[g, b],
                at(z, cq, xq),
            )

    far = [2, nx + 2, 1, nx + 1, 3, nx + 3, nx]

    def experts(g):
        for q in range(1, plane):
            arrived(rb.at[g, q * group_rows : (q + 1) * group_rows, :], drecv.at[g, q])
        taken = rb[g]
        hidden = (silu(dot(taken, eg[...])) * dot(taken, eu[...])).astype(BF16)
        for ch in range(NCH):
            cols = slice(ch * cw, (ch + 1) * cw)
            made = dot(hidden, ed[:, cols]).astype(BF16)
            cb[g, 0:group_rows, cols] = made[0:group_rows]
            eo[g, group_rows:, cols] = made[group_rows:]
        for q in far:
            cq, xq = mate(q)
            b = back(q)
            send(
                eo.at[g, q * group_rows : (q + 1) * group_rows, :],
                cb.at[g, b * group_rows : (b + 1) * group_rows, :],
                csend.at[g, q],
                crecv.at[g, b],
                at(z, cq, xq),
            )

    def combine(g):
        for q in range(1, plane):
            arrived(cb.at[g, q * group_rows : (q + 1) * group_rows, :], crecv.at[g, q])
        used = (PER + 1) * rows
        mix = com[g, 0:used, :]
        for ch in range(NCH):
            cols = slice(ch * cw, (ch + 1) * cw)
            summed = dot(mix, cb[g, :, cols])
            if g == 0:
                own[:, cols] = summed[0:rows]
            else:
                own[:, cols] = own[:, cols] + summed[0:rows]
            part[g * PER * rows : (g + 1) * PER * rows, cols] = summed[rows:used]

    gather_step(1)
    shared_expert()
    gather_step(2)
    gather_step(3)
    dispatch(0)
    gather_step(4)
    gather_step(5)
    dispatch(1)
    gather_step(6)
    load_eg.wait()
    load_eu.wait()
    load_ed.wait()
    experts(0)
    gather_step(7)
    gather_step(8)
    dispatch(2)
    experts(1)
    combine(0)
    experts(2)
    combine(1)
    combine(2)

    def brings(direction, step, ch):
        return step > 1 or (ch < NCH // 2) == (direction == 0)

    for step in range(1, half + 1):
        distance = half + 1 - step
        for ch in range(NCH):
            cols = slice(ch * cw, (ch + 1) * cw)
            for direction in range(2):
                if not brings(direction, step, ch):
                    continue
                s = slot[distance if direction == 0 else -distance]
                value = part[(s - 1) * rows : s * rows, cols]
                if step > 1 and brings(direction, step - 1, ch):
                    arrived(rsr.at[direction, step - 2, ch], rrecv.at[direction, step - 2, ch])
                    value = value + rsr[direction, step - 2, ch].astype(F32)
                rss[direction, step - 1, ch] = value.astype(BF16)
                send(
                    rss.at[direction, step - 1, ch],
                    rsr.at[direction, step - 1, ch],
                    rsend.at[direction, step - 1, ch],
                    rrecv.at[direction, step - 1, ch],
                    at(zs[direction], c, x),
                )

    base = stream[...] + shp[0:rows, :].astype(F32)
    for dx in range(1, nx):
        arrived(shr.at[dx], srecv.at[dx])
        base = base + shr[dx].astype(F32)
    stream[...] = base + own[...]
    for ch in range(NCH):
        cols = slice(ch * cw, (ch + 1) * cw)
        value = stream[:, cols]
        for direction in range(2):
            arrived(rsr.at[direction, half - 1, ch], rrecv.at[direction, half - 1, ch])
            value = value + rsr[direction, half - 1, ch].astype(F32)
        out_ref[:, cols] = value.astype(BF16)
    for copy in sent:
        copy.wait_send()


def body(nz, nx, *args):
    (
        query_rows,
        key_rows,
        value_rows,
        sink_logit,
        out_weight,
        residual,
        norm_gain,
        routes,
        gate_weights,
        expert_gate,
        expert_up,
        expert_down,
        shared_gate,
        shared_up,
        shared_down,
    ) = args
    rows, width = residual.shape
    span = query_rows.shape[0]
    half = nz // 2
    plane = 2 * nx
    groups = (nz - 1) // PER
    group_rows = PER * CAP + 1
    cw = width // NCH
    ff = expert_gate.shape[2]
    unit = shared_gate.shape[1]
    dma = pltpu.SemaphoreType.DMA
    vm = pltpu.VMEM
    scratch = [
        vm((span, query_rows.shape[1]), BF16),
        vm((2, 3 * span, key_rows.shape[1]), BF16),
        vm(out_weight.shape, BF16),
        vm((rows, width), BF16),
        vm((width, ff), BF16),
        vm((width, ff), BF16),
        vm((ff, width), BF16),
        vm((width, 2 * unit), BF16),
        vm((unit, width), BF16),
        vm((span, query_rows.shape[1]), BF16),
        vm((span, width), BF16),
        vm((nx, rows, width), BF16),
        vm((rows, width), F32),
        vm((nx * rows, width), BF16),
        vm((nx * rows, width), BF16),
        vm((nx, rows, width), BF16),
        vm((NCH, nz * rows, cw), BF16),
        vm((nz, 16, 128), F32),
        vm((groups, plane * group_rows, 256), BF16),
        vm((groups, 256, plane * group_rows), BF16),
        vm((groups, plane * group_rows, width), BF16),
        vm((groups, plane * group_rows, width), BF16),
        vm((groups, plane * group_rows, width), BF16),
        vm((groups, plane * group_rows, width), BF16),
        vm(((nz - 1) * rows, width), F32),
        vm((rows, width), F32),
        vm((2, half, NCH, rows, cw), BF16),
        vm((2, half, NCH, rows, cw), BF16),
        dma((11,)),
        dma((2,)),
        dma((2,)),
        dma((nx,)),
        dma((nx,)),
        dma((nx,)),
        dma((nx,)),
        dma((nx,)),
        dma((nx,)),
        dma((2, half, NCH)),
        dma((nz, NCH)),
        dma((2, half)),
        dma((nz,)),
        dma((groups, plane)),
        dma((groups, plane)),
        dma((groups, plane)),
        dma((groups, plane)),
        dma((2, half, NCH)),
        dma((2, half, NCH)),
    ]
    hbm = pl.BlockSpec(memory_space=pl.ANY)
    vmem = pl.BlockSpec(memory_space=pltpu.VMEM)
    smem = pl.BlockSpec(memory_space=pltpu.SMEM)
    return pl.pallas_call(
        functools.partial(kernel, nz, nx),
        out_shape=jax.ShapeDtypeStruct((rows, width), BF16),
        in_specs=[
            hbm,
            hbm,
            hbm,
            smem,
            hbm,
            hbm,
            vmem,
            vmem,
            vmem,
            hbm,
            hbm,
            hbm,
            hbm,
            hbm,
            hbm,
        ],
        out_specs=vmem,
        scratch_shapes=scratch,
        compiler_params=pltpu.CompilerParams(
            collective_id=0, has_side_effects=True, vmem_limit_bytes=60 * 1024 * 1024
        ),
    )(
        query_rows,
        key_rows,
        value_rows,
        sink_logit,
        out_weight,
        residual,
        norm_gain.reshape(1, width),
        routes,
        gate_weights,
        expert_gate,
        expert_up,
        expert_down,
        shared_gate,
        shared_up,
        shared_down,
    )


def solution(mesh):
    placed = (
        P(("grp", "sp"), "tp"),
        P(("grp", "sp"), "tp"),
        P(("grp", "sp"), "tp"),
        P("tp"),
        P("tp", None),
        P(("grp", "sp", "tp"), None),
        P(),
        P(("grp", "sp", "tp"), None),
        P(("grp", "sp", "tp"), None),
        P(("sp", "tp"), None, None),
        P(("sp", "tp"), None, None),
        P(("sp", "tp"), None, None),
        P(None, "tp"),
        P(None, "tp"),
        P("tp", None),
    )
    return jax.shard_map(
        functools.partial(body, mesh.shape["sp"] // 2, mesh.shape["tp"]),
        mesh=mesh,
        in_specs=placed,
        out_specs=P(("grp", "sp", "tp"), None),
        check_vma=False,
    )
```

time: 322 us -> 125 us (0.39)
  waiting for transfers between devices: 195 us -> 0 us
  Pallas kernels: 0 us -> 121 us
  starting transfers between devices: 64.7 us -> 0 us
  local copies, waits for them, and re-layouts: 36.8 us -> 4.3 us
  matrix products: 14.8 us -> 0 us
  other arithmetic: 7.61 us -> 0 us
    all_to_all x5 -> x0, waiting for transfers between devices: 195 us -> none  [the longest x1 94.8 us: body(): lax.all_to_all(result.reshape(incoming.shape), ('sp', 'tp'), split_axis=0...]
    pallas_call x0 -> x1, Pallas kernels: none -> 121 us  [body(): pl.pallas_call(functools.partial(kernel, nz, nx), out_shape=jax.ShapeDtyp...]
    all_to_all x5 -> x0, starting transfers between devices: 61.6 us -> none  [the longest x1 36.1 us: body(): lax.all_to_all(outgoing, ('sp', 'tp'), split_axis=0, concat_axis=0, tiled...]
    reshape x5 -> x0, local copies, waits for them, and re-layouts: 20.5 us -> none  [the longest x1 5.15 us: body(): padded_rows[slot_token].reshape(experts_all, capacity, model_width)]
    dot_general x7 -> x0, matrix products: 14.8 us -> none  [the longest x1 5.3 us: body(): jnp.dot(hidden, expert_down[0], preferred_element_type=jnp.float32)]
    gather x2 -> x0, local copies, waits for them, and re-layouts: 7.53 us -> none  [the longest x1 4.42 us: body(): gathered_copies = returned[target_slot].reshape(tok_rows, TOPK, model_width)]
    reduce_sum x6 -> x0, other arithmetic: 3.64 us -> none  [the longest x1 2.33 us: body(): jnp.sum(gate_weights[:, :, None] * gathered_copies.astype(jnp.float32), a...]
  transfers between devices with their start and end apart: 7 -> 0, of which waited for: 5 -> 0; matrix products, arithmetic and copies ran while one was open for 12% -> 0% of each run, Pallas kernels for 0% -> 0%
where the time goes in v1:
time: 125 us
  Pallas kernels  121 us (97%)
  local copies, waits for them, and re-layouts  4.3 us (3%)
    pallas_call x1, Pallas kernels, body(): pl.pallas_call(functools.partial(kernel, nz, nx), out_shape=jax.ShapeDtyp...  121 us
    unnamed x3, local copies, waits for them, and re-layouts  4.3 us

profile of v1, /device:TPU:40, one launch (start us, length us, event | category | flops | bytes accessed | tf_op | source)
XLA Modules:
  0.0 125.0 jit_solution(13915078275227249307)
XLA Ops:
  0.0 1.4 %copy.16.routes_ref = s32[32,6]{1,0:T(8,128)} copy(s32[32,6]{0,1:T(8,128)} %param.22) | data formatting | bytes 1536 | tf_op args[7]
  1.4 1.4 %copy.17.gw_ref = f32[32,6]{1,0:T(8,128)} copy(f32[32,6]{0,1:T(8,128)} %param.23) | data formatting | bytes 1536 | tf_op args[8]
  2.7 120.7 %shard_map.145 = bf16[32,2048]{1,0:T(8,128)(2,1)} custom-call(bf16[128,256]{1,0:T(8,128)(2,1)} %q_hbm.1, bf16[128,128]{1,0:T(8,128)(2,1)} %k_hbm.1, bf16[128,128]{1,0:T(8,128)(2,1)} %v_hbm.1, f32[4]{0:T(128)} %sink_ref.1, bf16[256,2048]{1,0:T(8,128)(2,1)} %ow_hbm.1, bf16[32,2048]{1,0:T(8,128)(2,1)} %res_hbm.1, f32[1,2048]{1,0:T(1,128)} %bitcast.1, ...), custom_call_target="tpu_custom_call" | custom-call | tf_op jit(solution)/shard_map/pallas_call | solution.py:627
  123.4 1.6 %copy.19 = bf16[32,2048]{1,0:T(8,128)(2,1)} copy(bf16[32,2048]{1,0:T(8,128)(2,1)} %shard_map.145) | data formatting | bytes 262144

commit v2 on v1

--- a/solution.py
+++ b/solution.py
@@ -13,6 +13,7 @@
 CAP = 3
 NCH = 4
 PER = 5
+LAG = 0.45
 NORM_EPS = 1e-06
 MESH = pl.DeviceIdType.MESH
 F32 = jnp.float32
@@ -37,12 +38,12 @@
     q_hbm,
     k_hbm,
     v_hbm,
-    sink_ref,
+    sink_hbm,
     ow_hbm,
     res_hbm,
-    gain_ref,
-    routes_ref,
-    gw_ref,
+    gain_hbm,
+    routes_hbm,
+    gw_hbm,
     eg_hbm,
     eu_hbm,
     ed_hbm,
@@ -50,6 +51,10 @@
     su_hbm,
     sd_hbm,
     out_ref,
+    sinks,
+    gain,
+    ids,
+    gates,
     qb,
     kv,
     ow,
@@ -74,6 +79,7 @@
     rb,
     eo,
     cb,
+    acc,
     part,
     own,
     rsr,
@@ -95,6 +101,10 @@
     drecv,
     csend,
     crecv,
+    dsend2,
+    drecv2,
+    csend2,
+    crecv2,
     rsend,
     rrecv,
 ):
@@ -176,42 +186,19 @@
     load_k = load(k_hbm, kv.at[0, span : 2 * span])
     load_v = load(v_hbm, kv.at[1, span : 2 * span])
     load_q = load(q_hbm, qb)
+    load_ids = load(routes_hbm, ids)
+    load_gates = load(gw_hbm, gates)
+    load_sink = load(sink_hbm, sinks)
     load_ow = load(ow_hbm, ow)
     load_res = load(res_hbm, res)
+    load_gain = load(gain_hbm, gain)
     unit = sg_hbm.shape[1]
+    load_eg = load(eg_hbm.at[0], eg)
+    load_eu = load(eu_hbm.at[0], eu)
+    load_ed = load(ed_hbm.at[0], ed)
     load_sg = load(sg_hbm, wsh.at[:, 0:unit])
     load_su = load(su_hbm, wsh.at[:, unit : 2 * unit])
     load_sd = load(sd_hbm, sd)
-    load_eg = load(eg_hbm.at[0], eg)
-    load_eu = load(eu_hbm.at[0], eu)
-    load_ed = load(ed_hbm.at[0], ed)
-
-    lane = iota((rows, 128), 1)
-    ids = routes_ref[...]
-    gates = gw_ref[...]
-    hot = jnp.zeros((rows, 128), F32)
-    for k in range(TOPK):
-        hot = hot + jnp.where(lane == ids[:, k : k + 1], 1.0, 0.0)
-    below = jnp.where(iota((rows, rows), 0) > iota((rows, rows), 1), 1.0, 0.0)
-    before = dot(below.astype(BF16), hot.astype(BF16))
-    e_cols = jnp.full((rows, 128), -1.0, F32)
-    r_cols = jnp.zeros((rows, 128), F32)
-    g_cols = jnp.zeros((rows, 128), F32)
-    for k in range(TOPK):
-        e_k = ids[:, k : k + 1]
-        rank = jnp.sum(jnp.where(lane == e_k, before, 0.0), axis=1, keepdims=True)
-        here = lane == k
-        e_cols = jnp.where(here, e_k.astype(F32), e_cols)
-        r_cols = jnp.where(here, rank, r_cols)
-        g_cols = jnp.where(here, gates[:, k : k + 1], g_cols)
-    spread = jnp.where((lane & (rows - 1)) == iota((rows, 128), 0), 1.0, 0.0).astype(BF16)
-
-    def on_lanes(cols):
-        return dot(cols.T.astype(BF16), spread)[0:8]
-
-    g_high = g_cols.astype(BF16).astype(F32)
-    meta[0, 0:8, :] = 4.0 * on_lanes(e_cols) + on_lanes(r_cols)
-    meta[0, 8:16, :] = on_lanes(g_high) + on_lanes(g_cols - g_high)
 
     load_k.wait()
     load_v.wait()
@@ -222,6 +209,32 @@
     prv = {"sp": (sp + nsp - 1) % nsp, "tp": x}
     send(mine, kv.at[:, 0:span, :], hsend.at[0], hrecv.at[0], nxt)
     send(mine, kv.at[:, 2 * span : 3 * span, :], hsend.at[1], hrecv.at[1], prv)
+
+    load_ids.wait()
+    load_gates.wait()
+    lane = iota((rows, 128), 1)
+    spread = jnp.where((lane & (rows - 1)) == iota((rows, 128), 0), 1.0, 0.0).astype(BF16)
+    named = dot(ids[...].astype(F32).astype(BF16), spread)
+    rest = gates[...]
+    weighted = jnp.zeros((TOPK, 128), F32)
+    for _ in range(3):
+        high = rest.astype(BF16)
+        weighted = weighted + dot(high, spread)
+        rest = rest - high.astype(F32)
+    names = iota((128, 128), 0).astype(F32)
+    hot = jnp.zeros((128, 128), F32)
+    for k in range(TOPK):
+        hot = hot + jnp.where(names == named[k : k + 1, :], 1.0, 0.0)
+    sub, on = iota((128, 128), 0), iota((128, 128), 1)
+    earlier = jnp.where((sub < (on & (rows - 1))) & (sub < rows), 1.0, 0.0)
+    before = dot(hot.astype(BF16), earlier.astype(BF16))
+    meta[0] = jnp.full((16, 128), -4.0, F32)
+    for k in range(TOPK):
+        rank = jnp.sum(
+            jnp.where(names == named[k : k + 1, :], before, 0.0), axis=0, keepdims=True
+        )
+        meta[0, k : k + 1, :] = 4.0 * named[k : k + 1, :] + rank
+        meta[0, 8 + k : 9 + k, :] = weighted[k : k + 1, :]
 
     load_q.wait()
     lane_q = iota((span, 128), 1)
@@ -240,6 +253,7 @@
     open_ = (col_i >= row_i) & (col_i <= row_i + 2 * WINDOW) & (pos >= 0) & (pos < nsp * span)
     arrived(kv.at[:, 0:span, :], hrecv.at[0])
     arrived(kv.at[:, 2 * span : 3 * span, :], hrecv.at[1])
+    load_sink.wait()
     keys = kv[0]
     values = kv[1]
     results = []
@@ -248,7 +262,7 @@
             query, keys, (((1,), (1,)), ((), ())), preferred_element_type=F32
         ) * (HEAD**-0.5)
         scores = jnp.where(open_, scores, -jnp.inf)
-        sink = sink_ref[h]
+        sink = sinks[h]
         row_max = jnp.maximum(jnp.max(scores, axis=-1, keepdims=True), sink)
         shifted = jnp.exp(scores - row_max)
         denominator = jnp.exp(sink - row_max) + jnp.sum(shifted, axis=-1, keepdims=True)
@@ -279,6 +293,7 @@
             at(z, c, xq),
         )
     load_res.wait()
+    load_gain.wait()
     total = res[...].astype(F32) + pbuf[pl.ds(pl.multiple_of(x * rows, rows), rows), :].astype(F32)
     for dx in range(1, nx):
         arrived(precv.at[dx], pecv.at[dx])
@@ -286,7 +301,7 @@
         total = total + precv[dx].astype(F32)
     stream[...] = total
     scale = lax.rsqrt(jnp.mean(total * total, axis=-1, keepdims=True) + NORM_EPS)
-    normed = (total * scale * gain_ref[...]).astype(BF16)
+    normed = (total * scale * gain[...]).astype(BF16)
     slab[0:rows, :] = normed
     for ch in range(NCH):
         ag[ch, 0:rows, :] = normed[:, ch * cw : (ch + 1) * cw]
@@ -324,26 +339,32 @@
             at(zs[direction], c, x),
         )
 
-    def gather_step(step):
-        for ch in range(NCH):
-            for direction in range(2):
-                if carries(direction, step, ch):
-                    s = source(direction, step)
-                    arrived(block(ch, s), agrecv.at[s, ch])
-                    if step < half:
-                        forward(step + 1, ch, direction)
+    def gather_meta(step):
         for direction in range(2):
             if not (step == half and direction == 1):
-                s = source(direction, step)
-                arrived(meta.at[s], mrecv.at[s])
+                t = source(direction, step)
+                arrived(meta.at[t], mrecv.at[t])
                 if step < half:
                     forward_meta(step + 1, direction)
 
+    def gather_chunk(step, ch):
+        for direction in range(2):
+            if carries(direction, step, ch):
+                t = source(direction, step)
+                arrived(block(ch, t), agrecv.at[t, ch])
+                if step < half:
+                    forward(step + 1, ch, direction)
+
+    def gather_step(step):
+        gather_meta(step)
+        for ch in range(NCH):
+            gather_chunk(step, ch)
+
+    for direction in range(2):
+        forward_meta(1, direction)
     for ch in range(NCH):
         for direction in range(2):
             forward(1, ch, direction)
-    for direction in range(2):
-        forward_meta(1, direction)
     for dx in (2, 1, 3):
         there = (nx - dx) % nx
         send(
@@ -365,6 +386,8 @@
         for ch in range(NCH):
             cols = slice(ch * cw, (ch + 1) * cw)
             shp[:, cols] = dot(hidden, sd[:, cols]).astype(BF16)
+
+    def shared_out():
         for dx in (2, 1, 3):
             there = (nx - dx) % nx
             send(
@@ -420,69 +443,102 @@
             column = jnp.concatenate([turned[q][v] for q in range(plane)], axis=0)
             com[g, v * 128 : (v + 1) * 128, :] = column.T.astype(BF16)
 
-    def dispatch(g):
-        build(g)
-        choose = sel[g]
-        for ch in range(NCH):
-            cols = slice(ch * cw, (ch + 1) * cw)
-            first = ag[ch, 0:rows, :]
-            begin = (1 + PER * g) * rows
-            stack = jnp.concatenate(
-                [first, ag[ch, begin : begin + PER * rows, :], first, first], axis=0
-            )
-            picked = dot(choose, stack).astype(BF16)
-            rb[g, 0:group_rows, cols] = picked[0:group_rows]
-            sb[g, group_rows:, cols] = picked[group_rows:]
+    far = [2, nx + 2, 1, nx + 1, 3, nx + 3, nx]
+    final = groups - 1
+
+    def part_of(q):
+        return slice(q * group_rows, (q + 1) * group_rows)
+
+    def columns(ch):
+        return slice(ch * cw, (ch + 1) * cw)
+
+    def swap(g, ch, src, dst, ss, rs, ss2, rs2):
         for q in far:
             cq, xq = mate(q)
             b = back(q)
-            send(
-                sb.at[g, q * group_rows : (q + 1) * group_rows, :],
-                rb.at[g, b * group_rows : (b + 1) * group_rows, :],
-                dsend.at[g, q],
-                drecv.at[g, b],
-                at(z, cq, xq),
-            )
-
-    far = [2, nx + 2, 1, nx + 1, 3, nx + 3, nx]
+            if ch is None:
+                send(
+                    src.at[g, :, part_of(q), :],
+                    dst.at[g, :, part_of(b), :],
+                    ss.at[g, q],
+                    rs.at[g, b],
+                    at(z, cq, xq),
+                )
+            else:
+                send(
+                    src.at[g, ch, part_of(q), :],
+                    dst.at[g, ch, part_of(b), :],
+                    ss2.at[ch, q],
+                    rs2.at[ch, b],
+                    at(z, cq, xq),
+                )
+
+    def came(g, ch, dst, rs, rs2):
+        for q in range(1, plane):
+            if g < final:
+                arrived(dst.at[g, :, part_of(q), :], rs.at[g, q])
+            else:
+                arrived(dst.at[g, ch, part_of(q), :], rs2.at[ch, q])
+
+    def pick(g, ch):
+        first = ag[ch, 0:rows, :]
+        begin = (1 + PER * g) * rows
+        stack = jnp.concatenate(
+            [first, ag[ch, begin : begin + PER * rows, :], first, first], axis=0
+        )
+        picked = dot(sel[g], stack).astype(BF16)
+        rb[g, ch, 0:group_rows, :] = picked[0:group_rows]
+        sb[g, ch, group_rows:, :] = picked[group_rows:]
+
+    def dispatch(g):
+        build(g)
+        for ch in range(NCH):
+            pick(g, ch)
+        swap(g, None, sb, rb, dsend, drecv, dsend2, drecv2)
+
+    def enter(g, ch):
+        rows_in = rb[g, ch]
+        gate = dot(rows_in, eg[columns(ch), :])
+        up = dot(rows_in, eu[columns(ch), :])
+        if ch == 0:
+            acc[0] = gate
+            acc[1] = up
+        else:
+            acc[0] = acc[0] + gate
+            acc[1] = acc[1] + up
+
+    def leave(g, ch, hidden):
+        made = dot(hidden, ed[:, columns(ch)]).astype(BF16)
+        cb[g, ch, 0:group_rows, :] = made[0:group_rows]
+        eo[g, ch, group_rows:, :] = made[group_rows:]
 
     def experts(g):
-        for q in range(1, plane):
-            arrived(rb.at[g, q * group_rows : (q + 1) * group_rows, :], drecv.at[g, q])
-        taken = rb[g]
+        came(g, None, rb, drecv, drecv2)
+        taken = [rb[g, ch] for ch in range(NCH)]
+        taken = jnp.concatenate(taken, axis=1)
         hidden = (silu(dot(taken, eg[...])) * dot(taken, eu[...])).astype(BF16)
         for ch in range(NCH):
-            cols = slice(ch * cw, (ch + 1) * cw)
-            made = dot(hidden, ed[:, cols]).astype(BF16)
-            cb[g, 0:group_rows, cols] = made[0:group_rows]
-            eo[g, group_rows:, cols] = made[group_rows:]
-        for q in far:
-            cq, xq = mate(q)
-            b = back(q)
-            send(
-                eo.at[g, q * group_rows : (q + 1) * group_rows, :],
-                cb.at[g, b * group_rows : (b + 1) * group_rows, :],
-                csend.at[g, q],
-                crecv.at[g, b],
-                at(z, cq, xq),
-            )
-
-    def combine(g):
-        for q in range(1, plane):
-            arrived(cb.at[g, q * group_rows : (q + 1) * group_rows, :], crecv.at[g, q])
+            leave(g, ch, hidden)
+
+    def give_back(g, ch):
+        swap(g, ch, eo, cb, csend, crecv, csend2, crecv2)
+
+    def combine(g, ch):
         used = (PER + 1) * rows
-        mix = com[g, 0:used, :]
+        summed = dot(com[g, 0:used, :], cb[g, ch])
+        cols = columns(ch)
+        if g == 0:
+            own[:, cols] = summed[0:rows]
+        else:
+            own[:, cols] = own[:, cols] + summed[0:rows]
+        part[g * PER * rows : (g + 1) * PER * rows, cols] = summed[rows:used]
+
+    def combine_all(g):
+        came(g, None, cb, crecv, crecv2)
         for ch in range(NCH):
-            cols = slice(ch * cw, (ch + 1) * cw)
-            summed = dot(mix, cb[g, :, cols])
-            if g == 0:
-                own[:, cols] = summed[0:rows]
-            else:
-                own[:, cols] = own[:, cols] + summed[0:rows]
-            part[g * PER * rows : (g + 1) * PER * rows, cols] = summed[rows:used]
+            combine(g, ch)
 
     gather_step(1)
-    shared_expert()
     gather_step(2)
     gather_step(3)
     dispatch(0)
@@ -494,38 +550,61 @@
     load_eu.wait()
     load_ed.wait()
     experts(0)
+    give_back(0, None)
     gather_step(7)
-    gather_step(8)
-    dispatch(2)
+    gather_meta(8)
+    build(final)
+    for ch in range(NCH):
+        gather_chunk(8, ch)
+        pick(final, ch)
+        swap(final, ch, sb, rb, dsend, drecv, dsend2, drecv2)
     experts(1)
-    combine(0)
-    experts(2)
-    combine(1)
-    combine(2)
+    shared_expert()
+    combine_all(0)
+    for ch in range(NCH):
+        came(final, ch, rb, drecv, drecv2)
+        enter(final, ch)
+    hidden = (silu(acc[0]) * acc[1]).astype(BF16)
+    for ch in range(NCH):
+        leave(final, ch, hidden)
+        give_back(final, ch)
+    give_back(1, None)
+    shared_out()
 
     def brings(direction, step, ch):
         return step > 1 or (ch < NCH // 2) == (direction == 0)
 
-    for step in range(1, half + 1):
+    def reduce_chunk(step, ch):
         distance = half + 1 - step
-        for ch in range(NCH):
-            cols = slice(ch * cw, (ch + 1) * cw)
-            for direction in range(2):
-                if not brings(direction, step, ch):
-                    continue
-                s = slot[distance if direction == 0 else -distance]
-                value = part[(s - 1) * rows : s * rows, cols]
-                if step > 1 and brings(direction, step - 1, ch):
-                    arrived(rsr.at[direction, step - 2, ch], rrecv.at[direction, step - 2, ch])
-                    value = value + rsr[direction, step - 2, ch].astype(F32)
-                rss[direction, step - 1, ch] = value.astype(BF16)
-                send(
-                    rss.at[direction, step - 1, ch],
-                    rsr.at[direction, step - 1, ch],
-                    rsend.at[direction, step - 1, ch],
-                    rrecv.at[direction, step - 1, ch],
-                    at(zs[direction], c, x),
-                )
+        for direction in range(2):
+            if not brings(direction, step, ch):
+                continue
+            s = slot[distance if direction == 0 else -distance]
+            value = part[(s - 1) * rows : s * rows, columns(ch)]
+            if step > 1 and brings(direction, step - 1, ch):
+                arrived(rsr.at[direction, step - 2, ch], rrecv.at[direction, step - 2, ch])
+                value = value + rsr[direction, step - 2, ch].astype(F32)
+            rss[direction, step - 1, ch] = value.astype(BF16)
+            send(
+                rss.at[direction, step - 1, ch],
+                rsr.at[direction, step - 1, ch],
+                rsend.at[direction, step - 1, ch],
+                rrecv.at[direction, step - 1, ch],
+                at(zs[direction], c, x),
+            )
+
+    events = sorted(
+        (step + LAG * ch, step, ch) for step in range(1, half + 1) for ch in range(NCH)
+    )
+    merged = False
+    for _, step, ch in events:
+        if step == 1:
+            came(final, ch, cb, crecv, crecv2)
+            combine(final, ch)
+        if step == 4 and not merged:
+            combine_all(1)
+            merged = True
+        reduce_chunk(step, ch)
 
     base = stream[...] + shp[0:rows, :].astype(F32)
     for dx in range(1, nx):
@@ -573,6 +652,10 @@
     dma = pltpu.SemaphoreType.DMA
     vm = pltpu.VMEM
     scratch = [
+        pltpu.SMEM(sink_logit.shape, F32),
+        vm((1, width), F32),
+        vm((TOPK, rows), jnp.int32),
+        vm((TOPK, rows), F32),
         vm((span, query_rows.shape[1]), BF16),
         vm((2, 3 * span, key_rows.shape[1]), BF16),
         vm(out_weight.shape, BF16),
@@ -593,15 +676,16 @@
         vm((nz, 16, 128), F32),
         vm((groups, plane * group_rows, 256), BF16),
         vm((groups, 256, plane * group_rows), BF16),
-        vm((groups, plane * group_rows, width), BF16),
-        vm((groups, plane * group_rows, width), BF16),
-        vm((groups, plane * group_rows, width), BF16),
-        vm((groups, plane * group_rows, width), BF16),
+        vm((groups, NCH, plane * group_rows, cw), BF16),
+        vm((groups, NCH, plane * group_rows, cw), BF16),
+        vm((groups, NCH, plane * group_rows, cw), BF16),
+        vm((groups, NCH, plane * group_rows, cw), BF16),
+        vm((2, plane * group_rows, ff), F32),
         vm(((nz - 1) * rows, width), F32),
         vm((rows, width), F32),
         vm((2, half, NCH, rows, cw), BF16),
         vm((2, half, NCH, rows, cw), BF16),
-        dma((11,)),
+        dma((15,)),
         dma((2,)),
         dma((2,)),
         dma((nx,)),
@@ -614,36 +698,23 @@
         dma((nz, NCH)),
         dma((2, half)),
         dma((nz,)),
-        dma((groups, plane)),
-        dma((groups, plane)),
-        dma((groups, plane)),
-        dma((groups, plane)),
+        dma((groups - 1, plane)),
+        dma((groups - 1, plane)),
+        dma((groups - 1, plane)),
+        dma((groups - 1, plane)),
+        dma((NCH, plane)),
+        dma((NCH, plane)),
+        dma((NCH, plane)),
+        dma((NCH, plane)),
         dma((2, half, NCH)),
         dma((2, half, NCH)),
     ]
     hbm = pl.BlockSpec(memory_space=pl.ANY)
     vmem = pl.BlockSpec(memory_space=pltpu.VMEM)
-    smem = pl.BlockSpec(memory_space=pltpu.SMEM)
     return pl.pallas_call(
         functools.partial(kernel, nz, nx),
         out_shape=jax.ShapeDtypeStruct((rows, width), BF16),
-        in_specs=[
-            hbm,
-            hbm,
-            hbm,
-            smem,
-            hbm,
-            hbm,
-            vmem,
-            vmem,
-            vmem,
-            hbm,
-            hbm,
-            hbm,
-            hbm,
-            hbm,
-            hbm,
-        ],
+        in_specs=[hbm] * 15,
         out_specs=vmem,
         scratch_shapes=scratch,
         compiler_params=pltpu.CompilerParams(
@@ -657,8 +728,8 @@
         out_weight,
         residual,
         norm_gain.reshape(1, width),
-        routes,
-        gate_weights,
+        routes.T,
+        gate_weights.T,
         expert_gate,
         expert_up,
         expert_down,

time: 125 us -> 116 us (0.928)
  Pallas kernels: 121 us -> 114 us
  local copies, waits for them, and re-layouts: 4.3 us -> 1.57 us
    pallas_call x1, Pallas kernels: 121 us -> 114 us  [body(): pl.pallas_call(functools.partial(kernel, nz, nx), out_shape=jax.ShapeDtyp...]
    unnamed x3 -> x1, local copies, waits for them, and re-layouts: 4.3 us -> 1.57 us
where the time goes in v2:
time: 116 us
  Pallas kernels  114 us (98%)
  local copies, waits for them, and re-layouts  1.57 us (1%)
    pallas_call x1, Pallas kernels, body(): pl.pallas_call(functools.partial(kernel, nz, nx), out_shape=jax.ShapeDtyp...  114 us

profile of v2, /device:TPU:40, one launch (start us, length us, event | category | flops | bytes accessed | tf_op | source)
XLA Modules:
  0.0 115.8 jit_solution(7464103300024152775)
XLA Ops:
  0.0 114.2 %shard_map.145 = bf16[32,2048]{1,0:T(8,128)(2,1)} custom-call(bf16[128,256]{1,0:T(8,128)(2,1)} %q_hbm.1, bf16[128,128]{1,0:T(8,128)(2,1)} %k_hbm.1, bf16[128,128]{1,0:T(8,128)(2,1)} %v_hbm.1, f32[4]{0:T(128)} %sink_hbm.1, bf16[256,2048]{1,0:T(8,128)(2,1)} %ow_hbm.1, bf16[32,2048]{1,0:T(8,128)(2,1)} %res_hbm.1, f32[1,2048]{1,0:T(1,128)} %bitcast.3, ...), custom_call_target="tpu_custom_call" | custom-call | tf_op jit(solution)/shard_map/pallas_call | solution.py:714
  114.2 1.6 %copy.17 = bf16[32,2048]{1,0:T(8,128)(2,1)} copy(bf16[32,2048]{1,0:T(8,128)(2,1)} %shard_map.145) | data formatting | bytes 262144

commit v3 on v2

--- a/solution.py
+++ b/solution.py
@@ -82,6 +82,7 @@
     acc,
     part,
     own,
+    staged,
     rsr,
     rss,
     lsem,
@@ -213,13 +214,15 @@
     load_ids.wait()
     load_gates.wait()
     lane = iota((rows, 128), 1)
-    spread = jnp.where((lane & (rows - 1)) == iota((rows, 128), 0), 1.0, 0.0).astype(BF16)
-    named = dot(ids[...].astype(F32).astype(BF16), spread)
+    line = iota((rows, 128), 0)
+    first_seg = jnp.where(lane == line, 1.0, 0.0).astype(BF16)
+    second_seg = jnp.where(lane == line + rows, 1.0, 0.0).astype(BF16)
+    named = dot(ids[...].astype(F32).astype(BF16), first_seg)
     rest = gates[...]
     weighted = jnp.zeros((TOPK, 128), F32)
     for _ in range(3):
         high = rest.astype(BF16)
-        weighted = weighted + dot(high, spread)
+        weighted = weighted + dot(high, second_seg)
         rest = rest - high.astype(F32)
     names = iota((128, 128), 0).astype(F32)
     hot = jnp.zeros((128, 128), F32)
@@ -228,13 +231,14 @@
     sub, on = iota((128, 128), 0), iota((128, 128), 1)
     earlier = jnp.where((sub < (on & (rows - 1))) & (sub < rows), 1.0, 0.0)
     before = dot(hot.astype(BF16), earlier.astype(BF16))
-    meta[0] = jnp.full((16, 128), -4.0, F32)
+    segment = iota((1, 128), 1) // rows
+    meta[0] = jnp.full((8, 128), -4.0, F32)
     for k in range(TOPK):
-        rank = jnp.sum(
-            jnp.where(names == named[k : k + 1, :], before, 0.0), axis=0, keepdims=True
+        name = named[k : k + 1, :]
+        rank = jnp.sum(jnp.where(names == name, before, 0.0), axis=0, keepdims=True)
+        meta[0, k : k + 1, :] = jnp.where(
+            segment == 0, 4.0 * name + rank, weighted[k : k + 1, :]
         )
-        meta[0, k : k + 1, :] = 4.0 * named[k : k + 1, :] + rank
-        meta[0, 8 + k : 9 + k, :] = weighted[k : k + 1, :]
 
     load_q.wait()
     lane_q = iota((span, 128), 1)
@@ -409,9 +413,11 @@
                 p = 4 * v + i
                 if p > PER:
                     continue
-                s = 0 if p == 0 else PER * g + p
-                code = jnp.where(seg8 == i, meta[s, 0:8, :], code)
-                gate = jnp.where(seg8 == i, meta[s, 8:16, :], gate)
+                tile = meta[0 if p == 0 else PER * g + p]
+                ahead = pltpu.roll(tile, i * rows, 1) if i > 0 else tile
+                code = jnp.where(seg8 == i, ahead, code)
+                ahead = pltpu.roll(tile, (i + 3) % 4 * rows, 1) if i != 1 else tile
+                gate = jnp.where(seg8 == i, ahead, gate)
             codes.append(code)
             gws.append(gate)
         rr = iota((group_rows, 128), 0)
@@ -527,7 +533,7 @@
         used = (PER + 1) * rows
         summed = dot(com[g, 0:used, :], cb[g, ch])
         cols = columns(ch)
-        if g == 0:
+        if g == final:
             own[:, cols] = summed[0:rows]
         else:
             own[:, cols] = own[:, cols] + summed[0:rows]
@@ -550,7 +556,6 @@
     load_eu.wait()
     load_ed.wait()
     experts(0)
-    give_back(0, None)
     gather_step(7)
     gather_meta(8)
     build(final)
@@ -560,7 +565,6 @@
         swap(final, ch, sb, rb, dsend, drecv, dsend2, drecv2)
     experts(1)
     shared_expert()
-    combine_all(0)
     for ch in range(NCH):
         came(final, ch, rb, drecv, drecv2)
         enter(final, ch)
@@ -569,6 +573,7 @@
         leave(final, ch, hidden)
         give_back(final, ch)
     give_back(1, None)
+    give_back(0, None)
     shared_out()
 
     def brings(direction, step, ch):
@@ -596,14 +601,15 @@
     events = sorted(
         (step + LAG * ch, step, ch) for step in range(1, half + 1) for ch in range(NCH)
     )
-    merged = False
+    merged = []
     for _, step, ch in events:
         if step == 1:
             came(final, ch, cb, crecv, crecv2)
             combine(final, ch)
-        if step == 4 and not merged:
-            combine_all(1)
-            merged = True
+        for g, least in ((1, 4), (0, 6)):
+            if step == least and g not in merged:
+                combine_all(g)
+                merged.append(g)
         reduce_chunk(step, ch)
 
     base = stream[...] + shp[0:rows, :].astype(F32)
@@ -617,9 +623,12 @@
         for direction in range(2):
             arrived(rsr.at[direction, half - 1, ch], rrecv.at[direction, half - 1, ch])
             value = value + rsr[direction, half - 1, ch].astype(F32)
-        out_ref[:, cols] = value.astype(BF16)
+        staged[:, cols] = value.astype(BF16)
+        load(staged.at[:, cols], out_ref.at[:, cols])
     for copy in sent:
         copy.wait_send()
+    for copy in loads[-NCH:]:
+        copy.wait()
 
 
 def body(nz, nx, *args):
@@ -673,7 +682,7 @@
         vm((nx * rows, width), BF16),
         vm((nx, rows, width), BF16),
         vm((NCH, nz * rows, cw), BF16),
-        vm((nz, 16, 128), F32),
+        vm((nz, 8, 128), F32),
         vm((groups, plane * group_rows, 256), BF16),
         vm((groups, 256, plane * group_rows), BF16),
         vm((groups, NCH, plane * group_rows, cw), BF16),
@@ -683,9 +692,10 @@
         vm((2, plane * group_rows, ff), F32),
         vm(((nz - 1) * rows, width), F32),
         vm((rows, width), F32),
+        vm((rows, width), BF16),
         vm((2, half, NCH, rows, cw), BF16),
         vm((2, half, NCH, rows, cw), BF16),
-        dma((15,)),
+        dma((15 + NCH,)),
         dma((2,)),
         dma((2,)),
         dma((nx,)),
@@ -710,12 +720,11 @@
         dma((2, half, NCH)),
     ]
     hbm = pl.BlockSpec(memory_space=pl.ANY)
-    vmem = pl.BlockSpec(memory_space=pltpu.VMEM)
     return pl.pallas_call(
         functools.partial(kernel, nz, nx),
         out_shape=jax.ShapeDtypeStruct((rows, width), BF16),
         in_specs=[hbm] * 15,
-        out_specs=vmem,
+        out_specs=hbm,
         scratch_shapes=scratch,
         compiler_params=pltpu.CompilerParams(
             collective_id=0, has_side_effects=True, vmem_limit_bytes=60 * 1024 * 1024

time: 116 us -> 112 us (0.966)
  Pallas kernels: 114 us -> 110 us
    pallas_call x1, Pallas kernels: 114 us -> 110 us  [body(): pl.pallas_call(functools.partial(kernel, nz, nx), out_shape=jax.ShapeDtyp...]
where the time goes in v3:
time: 112 us
  Pallas kernels  110 us (98%)
  local copies, waits for them, and re-layouts  1.57 us (1%)
    pallas_call x1, Pallas kernels, body(): pl.pallas_call(functools.partial(kernel, nz, nx), out_shape=jax.ShapeDtyp...  110 us

profile of v3, /device:TPU:40, one launch (start us, length us, event | category | flops | bytes accessed | tf_op | source)
XLA Modules:
  0.0 111.9 jit_solution(15985824363430016885)
XLA Ops:
  0.0 110.3 %shard_map.145 = bf16[32,2048]{1,0:T(8,128)(2,1)} custom-call(bf16[128,256]{1,0:T(8,128)(2,1)} %q_hbm.1, bf16[128,128]{1,0:T(8,128)(2,1)} %k_hbm.1, bf16[128,128]{1,0:T(8,128)(2,1)} %v_hbm.1, f32[4]{0:T(128)} %sink_hbm.1, bf16[256,2048]{1,0:T(8,128)(2,1)} %ow_hbm.1, bf16[32,2048]{1,0:T(8,128)(2,1)} %res_hbm.1, f32[1,2048]{1,0:T(1,128)} %bitcast.3, ...), custom_call_target="tpu_custom_call" | custom-call | tf_op jit(solution)/shard_map/pallas_call | solution.py:723
  110.3 1.6 %copy.17 = bf16[32,2048]{1,0:T(8,128)(2,1)} copy(bf16[32,2048]{1,0:T(8,128)(2,1)} %shard_map.145) | data formatting | bytes 262144
